TPU v7x, 32 devices: a whole 2x2x4 slice. The times are simulated.
32 devices in a mesh: sp: 4 (over z), fs: 4 (over y, core), tp: 2 (over x).
Axes of the slice: x: 2, y: 2, z: 4, core: 2. Of those that a mesh axis runs over, the one named last changes fastest.
Arguments:
- tokens: bfloat16 [8, 2048, 2048], P('fs', ('sp', 'tp')), may hold values from -6 to 6
- norm_gain: float32 [2048], replicated, may hold values from 0.1 to 1.9
- w_pool_in: bfloat16 [2048, 1024], P('fs', 'tp'), may hold values from -0.125 to 0.125
- pool_mix: bfloat16 [8, 128, 128], replicated, may hold values from -0.5 to 0.5
- pool_scale: float32 [1024], replicated, may hold values from 0.1 to 1.9
- w_query: bfloat16 [2048, 1024], P('fs', 'tp'), may hold values from -0.13258252 to 0.13258252
- w_key: bfloat16 [2048, 1024], P('fs', 'tp'), may hold values from -0.508233 to 0.508233
- w_value: bfloat16 [2048, 1024], P('fs', 'tp'), may hold values from -0.125 to 0.125
- gate_cache: float32 [8, 8, 2048], P('fs', 'tp'), may hold values from -258 to 0, as said below
- w_out_pool: bfloat16 [1024, 2048], P('tp', 'fs'), may hold values from -0.125 to 0.125
- w_out_attn: bfloat16 [1024, 2048], P('tp', 'fs'), may hold values from -0.75 to 0.75
Outputs:
- mixed: bfloat16 [8, 2048, 2048], P('fs', ('sp', 'tp'))
Inputs may be any that keep to these rules, and one draw needn't show every extreme that they name: `gate_cache`: each head's values never rise along the positions.
All inputs are finite; a program needn't handle non-finite values.
Results may differ from a plain program's by a relative error of at most 0.014.
Values may be sent and summed in bfloat16 or wider, within the bound.
A program may use at most 128 MiB of HBM per device.

v0:
```python
import jax
import jax.numpy as jnp
from jax import lax
from jax.sharding import PartitionSpec as P

HEAD_DIM = 128
GROUP_WIDTH = 128
norm_eps = 1e-06
widest = 16
masked_score = -1e30


def shifted(x, axis, by):
    length = lax.axis_size(axis)
    pairs = [(i, i + by) for i in range(length) if 0 <= i + by < length]
    return lax.ppermute(x, axis, pairs)


def window_sums(extended):
    outcome = []
    current = extended
    offset = 1
    for doubling in range(4):
        padding = jnp.zeros((offset, extended.shape[1]), jnp.float32)
        current = current + jnp.concatenate([padding, current[:-offset]], axis=0)
        offset = offset * 2
        outcome.append(current[widest - 1 :])
    return outcome


def pool_branch(projected, border, first_group, first_position, mixing, scaling):
    row_count = projected.shape[0]
    channels = projected.shape[1]
    widened = projected.astype(jnp.float32)
    totals = window_sums(jnp.concatenate([border.astype(jnp.float32), widened], axis=0))
    token_positions = first_position + jnp.arange(row_count)
    window_index = (first_group + jnp.arange(channels) // GROUP_WIDTH) % 4
    averaged = jnp.zeros((row_count, channels), jnp.float32)
    for doubling in range(4):
        counted = jnp.minimum(token_positions + 1, 2 ** (doubling + 1)).astype(jnp.float32)
        picked = (window_index == doubling).astype(jnp.float32)
        averaged = averaged + picked[None, :] * totals[doubling] / counted[:, None]
    departure = (averaged - widened).astype(jnp.bfloat16)
    group_count = channels // GROUP_WIDTH
    mixed_rows = jnp.einsum(
        "tgc,gcd->tgd",
        departure.reshape(row_count, group_count, GROUP_WIDTH),
        mixing,
        preferred_element_type=jnp.float32,
    )
    return (mixed_rows.reshape(row_count, channels) * scaling[None, :]).astype(jnp.bfloat16)


def on_device(
    tokens,
    norm_gain,
    w_pool_in,
    pool_mix,
    pool_scale,
    w_query,
    w_key,
    w_value,
    gate_cache,
    w_out_pool,
    w_out_attn,
):
    tp_index = lax.axis_index("tp")
    tp_count = lax.axis_size("tp")
    seq_count = tokens.shape[0]
    own_count = tokens.shape[1]
    token_count = own_count * tp_count
    first_position = lax.axis_index("sp") * token_count
    own_rows = tokens.astype(jnp.float32)
    normed = (
        own_rows
        * lax.rsqrt(jnp.mean(own_rows * own_rows, axis=-1, keepdims=True) + norm_eps)
        * norm_gain[None, None, :]
    ).astype(jnp.bfloat16)
    pool_full, query_full, key_full, value_full, out_pool_full, out_attn_full = (
        lax.all_gather(w_pool_in, "fs", axis=0, tiled=True),
        lax.all_gather(w_query, "fs", axis=0, tiled=True),
        lax.all_gather(w_key, "fs", axis=0, tiled=True),
        lax.all_gather(w_value, "fs", axis=0, tiled=True),
        lax.all_gather(w_out_pool, "fs", axis=1, tiled=True),
        lax.all_gather(w_out_attn, "fs", axis=1, tiled=True),
    )
    pool_cols = w_pool_in.shape[1]
    attn_cols = w_query.shape[1]
    shard_rows = lax.all_gather(normed, "tp", axis=1, tiled=True)
    projected = jnp.concatenate(
        [
            jnp.dot(shard_rows, pool_full, preferred_element_type=jnp.float32).astype(jnp.bfloat16),
            jnp.dot(shard_rows, query_full, preferred_element_type=jnp.float32).astype(
                jnp.bfloat16
            ),
            jnp.dot(shard_rows, key_full, preferred_element_type=jnp.float32).astype(jnp.bfloat16),
            jnp.dot(shard_rows, value_full, preferred_element_type=jnp.float32).astype(
                jnp.bfloat16
            ),
        ],
        axis=2,
    )
    pool_in = projected[:, :, :pool_cols]
    query_proj = projected[:, :, pool_cols : pool_cols + attn_cols]
    key_proj = projected[:, :, pool_cols + attn_cols : pool_cols + 2 * attn_cols]
    value_proj = projected[:, :, pool_cols + 2 * attn_cols :]
    group_local = pool_cols // GROUP_WIDTH
    mixing = lax.dynamic_slice_in_dim(pool_mix, tp_index * group_local, group_local, 0)
    scaling = lax.dynamic_slice_in_dim(pool_scale, tp_index * pool_cols, pool_cols, 0)
    borders = shifted(pool_in[:, token_count - (widest - 1) :], "sp", 1)
    pool_out = jnp.stack(
        [
            pool_branch(
                pool_in[member],
                borders[member],
                tp_index * group_local,
                first_position,
                mixing,
                scaling,
            )
            for member in range(seq_count)
        ],
        axis=0,
    )
    head_count = attn_cols // HEAD_DIM
    query_heads = query_proj.reshape(seq_count, token_count, head_count, HEAD_DIM)
    query_gates = jnp.transpose(
        lax.dynamic_slice_in_dim(gate_cache, first_position, token_count, 2), (0, 2, 1)
    )
    query_positions = first_position + jnp.arange(token_count)
    last_position = first_position + token_count - 1
    score_scale = HEAD_DIM ** (-0.5)
    start_state = (
        jnp.full((seq_count, token_count, head_count), masked_score, jnp.float32),
        jnp.zeros((seq_count, token_count, head_count), jnp.float32),
        jnp.zeros((seq_count, token_count, head_count, HEAD_DIM), jnp.float32),
    )
    key_shard = lax.all_gather(key_proj, "sp", axis=1, tiled=True)
    value_shard = lax.all_gather(value_proj, "sp", axis=1, tiled=True)
    key_total = key_shard.shape[1]
    block_rows = 512

    def one_block(block_state, block_index):
        key_start = block_index * block_rows

        def compute(inner_state):
            running_top, running_sum, running_out = inner_state
            key_block = lax.dynamic_slice_in_dim(key_shard, block_index * block_rows, block_rows, 1)
            value_block = lax.dynamic_slice_in_dim(
                value_shard, block_index * block_rows, block_rows, 1
            )
            key_block = key_block.reshape(seq_count, block_rows, head_count, HEAD_DIM)
            value_block = value_block.reshape(seq_count, block_rows, head_count, HEAD_DIM)
            key_gates = lax.dynamic_slice_in_dim(gate_cache, key_start, block_rows, 2)
            scores = (
                jnp.einsum(
                    "sqhd,skhd->sqhk", query_heads, key_block, preferred_element_type=jnp.float32
                )
                * score_scale
            )
            scores = scores + query_gates[:, :, :, None] - key_gates[:, None, :, :]
            allowed = ((key_start + jnp.arange(block_rows))[None, :] <= query_positions[:, None])[
                None, :, None, :
            ]
            scores = jnp.where(allowed, scores, masked_score)
            new_top = jnp.maximum(running_top, jnp.max(scores, axis=3))
            weights = jnp.where(allowed, jnp.exp(scores - new_top[:, :, :, None]), 0.0)
            shrink = jnp.exp(running_top - new_top)
            running_sum = running_sum * shrink + jnp.sum(weights, axis=3)
            running_out = running_out * shrink[:, :, :, None] + jnp.einsum(
                "sqhk,skhd->sqhd",
                weights.astype(jnp.bfloat16),
                value_block,
                preferred_element_type=jnp.float32,
            )
            return (new_top, running_sum, running_out)

        def unchanged(inner_state):
            return inner_state

        return (lax.cond(key_start <= last_position, compute, unchanged, block_state), None)

    result, unused = lax.scan(one_block, start_state, jnp.arange(key_total // block_rows))
    final_top, final_sum, final_out = result
    attn_out = (
        (final_out / final_sum[:, :, :, None])
        .astype(jnp.bfloat16)
        .reshape(seq_count, token_count, attn_cols)
    )
    pool_flat = jnp.transpose(
        pool_out.reshape(seq_count, tp_count, own_count, pool_cols), (1, 0, 2, 3)
    ).reshape(tp_count * seq_count * own_count, pool_cols)
    attn_flat = jnp.transpose(
        attn_out.reshape(seq_count, tp_count, own_count, attn_cols), (1, 0, 2, 3)
    ).reshape(tp_count * seq_count * own_count, attn_cols)
    summed = lax.psum_scatter(
        (
            jnp.dot(pool_flat, out_pool_full, preferred_element_type=jnp.float32)
            + jnp.dot(attn_flat, out_attn_full, preferred_element_type=jnp.float32)
        ).astype(jnp.bfloat16),
        "tp",
        scatter_dimension=0,
        tiled=True,
    ).astype(jnp.float32)
    return summed.astype(jnp.bfloat16).reshape(seq_count, own_count, summed.shape[1])


def solution(mesh):
    placed = (
        P("fs", ("sp", "tp"), None),
        P(),
        P("fs", "tp"),
        P(),
        P(),
        P("fs", "tp"),
        P("fs", "tp"),
        P("fs", "tp"),
        P("fs", "tp", None),
        P("tp", "fs"),
        P("tp", "fs"),
    )
    return jax.shard_map(
        on_device,
        mesh=mesh,
        in_specs=placed,
        out_specs=P("fs", ("sp", "tp"), None),
        check_vma=False,
    )
```

profile of v0, /device:TPU:0, one launch (start us, length us, event | category | flops | bytes accessed | tf_op | source)
XLA Modules:
  0.0 483.2 jit_solution(8892311270368384525)
XLA Ops:
  14.4 19.8 %all-gather.16.cloned.1.call-done = bf16[2048,512]{1,0:T(8,128)(2,1)} async-done(((bf16[512,512]{1,0:T(8,128)(2,1)}), bf16[2048,512]{1,0:T(8,128)(2,1)}) %all-gather.16.cloned.1.call-update) | async-done | bytes 2097168 | tf_op jit(solution)/shard_map/all_gather | solution.py:82
  34.2 58.3 %all-gather.10.cloned.1.call-done = bf16[2,512,2048]{2,1,0:T(8,128)(2,1)} async-done(((bf16[2,256,2048]{2,1,0:T(8,128)(2,1)}), bf16[2,512,2048]{2,1,0:T(8,128)(2,1)}) %all-gather.10.cloned.1.call-update) | async-done | bytes 4194320 | tf_op jit(solution)/shard_map/all_gather | solution.py:89
  92.5 6.2 %fusion.29 = bf16[2,512,512]{2,1,0:T(8,128)(2,1)} fusion(bf16[2,512,2048]{2,1,0:T(8,128)(2,1)} %all-gather.10.cloned.1.call-done, bf16[2048,512]{1,0:T(8,128)(2,1)} %all-gather.16.cloned.1.call-done), kind=kOutput, calls=%fused_computation.42 | convolution fusion | flops 2148007936 | bytes 7340032 | tf_op jit(solution)/shard_map/dot_general | solution.py:96
  98.8 17.9 %all-gather.22.cloned.1.call-done = bf16[2048,512]{1,0:T(8,128)(2,1)} async-done(((bf16[512,512]{1,0:T(8,128)(2,1)}), bf16[2048,512]{1,0:T(8,128)(2,1)}) %all-gather.22.cloned.1.call-update) | async-done | bytes 2097168 | tf_op jit(solution)/shard_map/all_gather | solution.py:83
  116.7 6.2 %fusion.35 = bf16[2,512,512]{2,1,0:T(8,128)(2,1)} fusion(bf16[2,512,2048]{2,1,0:T(8,128)(2,1)} %all-gather.10.cloned.1.call-done, bf16[2048,512]{1,0:T(8,128)(2,1)} %all-gather.22.cloned.1.call-done), kind=kOutput, calls=%fused_computation.44 | convolution fusion | flops 2148007936 | bytes 7340032 | tf_op jit(solution)/shard_map/dot_general | solution.py:97
  124.4 16.3 %all-gather.12.cloned.1.call-done = bf16[2048,512]{1,0:T(8,128)(2,1)} async-done(((bf16[512,512]{1,0:T(8,128)(2,1)}), bf16[2048,512]{1,0:T(8,128)(2,1)}) %all-gather.12.cloned.1.call-update) | async-done | bytes 2097168 | tf_op jit(solution)/shard_map/all_gather | solution.py:80
  140.7 5.2 %fusion.26 = bf16[2,512,512]{2,1,0:T(8,128)(2,1)S(1)} fusion(bf16[2,512,2048]{2,1,0:T(8,128)(2,1)} %all-gather.10.cloned.1.call-done, bf16[2048,512]{1,0:T(8,128)(2,1)} %all-gather.12.cloned.1.call-done), kind=kOutput, calls=%fused_computation.41 | convolution fusion | flops 2148007936 | bytes 7340032 | tf_op jit(solution)/shard_map/dot_general | solution.py:92
  145.9 4.0 collective-permute-start
  149.9 14.8 %all-gather.20.cloned.1.call-done = bf16[2048,512]{0,1:T(8,128)(2,1)} async-done(((bf16[512,512]{0,1:T(8,128)(2,1)}), bf16[2048,512]{0,1:T(8,128)(2,1)}) %all-gather.20.cloned.1.call-update) | async-done | bytes 2097168 | tf_op jit(solution)/shard_map/all_gather | solution.py:81
  164.7 6.2 %fusion.32 = bf16[2,512,512]{1,2,0:T(8,128)(2,1)} fusion(bf16[2,512,2048]{2,1,0:T(8,128)(2,1)} %all-gather.10.cloned.1.call-done, bf16[2048,512]{0,1:T(8,128)(2,1)} %all-gather.20.cloned.1.call-done), kind=kOutput, calls=%fused_computation.43 | convolution fusion | flops 2148007936 | bytes 7340032 | tf_op jit(solution)/shard_map/dot_general | solution.py:93
  176.3 2.9 fusion.67
  184.4 4.3 all-gather.14.cloned.1.call-done
  188.7 7.2 %fusion.79 = f32[1024,2048]{1,0:T(8,128)} fusion(bf16[1024,512]{1,0:T(8,128)(2,1)S(1)} %bitcast.129, bf16[512,2048]{1,0:T(8,128)(2,1)} %all-gather.14.cloned.1.call-done), kind=kOutput, calls=%fused_computation.123 | convolution fusion | flops 2147483648 | bytes 11534336 | tf_op jit(solution)/shard_map/dot_general | solution.py:198
  195.9 75.1 %all-gather.18.cloned.1.call-done = bf16[2,2048,512]{2,1,0:T(8,128)(2,1)} async-done(((bf16[2,512,512]{2,1,0:T(8,128)(2,1)}), bf16[2,2048,512]{2,1,0:T(8,128)(2,1)}) %all-gather.18.cloned.1.call-update) | async-done | bytes 4194320 | tf_op jit(solution)/shard_map/all_gather | solution.py:138
  271.0 6.3 %copy.38 = bf16[2,2048,512]{1,2,0:T(8,128)(2,1)} copy(bf16[2,2048,512]{2,1,0:T(8,128)(2,1)} %all-gather.18.cloned.1.call-done) | data formatting | bytes 8388608
  277.3 74.5 %all-gather.24.cloned.1.call-done = bf16[2,2048,512]{2,1,0:T(8,128)(2,1)} async-done(((bf16[2,512,512]{2,1,0:T(8,128)(2,1)}), bf16[2,2048,512]{2,1,0:T(8,128)(2,1)}) %all-gather.24.cloned.1.call-update) | async-done | bytes 4194320 | tf_op jit(solution)/shard_map/all_gather | solution.py:139
  351.9 6.3 %copy.40 = bf16[2,2048,512]{1,2,0:T(8,128)(2,1)} copy(bf16[2,2048,512]{2,1,0:T(8,128)(2,1)} %all-gather.24.cloned.1.call-done) | data formatting | bytes 8388608
  359.5 17.2 %while.15 = (s32[]{:T(128)}, f32[2,512,4]{1,2,0:T(4,128)S(1)}, f32[2,512,4]{1,2,0:T(4,128)S(1)}, f32[2,512,4,128]{1,3,2,0:T(8,128)S(1)}, s32[4]{0:T(128)S(1)}, /...) while((s32[]{:T(128)}, f32[2,512,4]{1,2,0:T(4,128)S(1)}, ...), condition=%wide.region_6.7_spmd.clone, body=%wide.region_1.6_spmd.clone.sunk | while | flops 1114907648 | bytes 38154664 | solution.py:183
  360.7 12.1 %conditional.3 = ((f32[2,512,4]{1,2,0:T(4,128)S(1)}, f32[2,512,4]{1,2,0:T(4,128)S(1)}, f32[2,512,4,128]{1,3,2,0:T(8,128)S(1)})) conditional(s32[]{:T(128)} %convert_element_type.217, (f32[2,512,4]{1,2,0:T(4,128)S(1)}, f32[2,512,4]{1,2,0:T(4,128)S(1)}, f32[2,512,4,128]{1,3,2,0:T(8,128)S(1)}) %tuple.49, (s32[]{:T(128)}, s32[]{:T(128)}, s32[]{:T(128)}, ...), branch_computations={%region_2.2_spmd, %region_3.5_spmd} | conditional | flops 1114907648 | bytes 38152320 | solution.py:181
  363.4 2.6 fusion.6
  366.0 3.2 fusion.5
  369.2 3.5 bitcast_add_fusion.1
  378.8 8.4 %add_convert_fusion = bf16[1024,2048]{1,0:T(8,128)(2,1)} fusion(f32[1024,2048]{1,0:T(8,128)} %fusion.79, bf16[1024,512]{1,0:T(8,128)(2,1)S(1)} %bitcast.130, bf16[512,2048]{1,0:T(8,128)(2,1)} %all-gather.26.cloned.1.call-done), kind=kOutput, calls=%fused_computation.22 | convolution fusion | flops 2151677952 | bytes 15728640 | tf_op jit(solution)/shard_map/dot_general | solution.py:199
  387.2 89.2 %reduce-scatter.2.cloned.1.call-done = bf16[512,2048]{1,0:T(8,128)(2,1)} async-done(((bf16[1024,2048]{1,0:T(8,128)(2,1)}), bf16[512,2048]{1,0:T(8,128)(2,1)}) %reduce-scatter.2.cloned.1.call-update) | async-done | bytes 2097168 | tf_op jit(solution)/shard_map/reduce_scatter | solution.py:196
  (96 shorter events, 27.4 us)
Async XLA Ops:
  6.5 172.7 %copy-start = (bf16[8,128,128]{2,1,0:T(8,128)(2,1)S(1)}, bf16[8,128,128]{2,1,0:T(8,128)(2,1)}, u32[]{:S(2)}) copy-start(bf16[8,128,128]{2,1,0:T(8,128)(2,1)} %param.18) | copy-start | bytes 786436
  6.5 2.9 copy-start.2
  6.5 2.9 copy-start.6
  6.5 27.7 %all-gather.16.cloned.1.call-start = ((), (), s32[]{:S(2)}) async-start(), calls=%async_computation.4 | async-start | bytes 2621440 | tf_op jit(solution)/shard_map/all_gather | solution.py:82
  7.3 85.2 %all-gather.10.cloned.1.call-start = ((), (), s32[]{:S(2)}) async-start(), calls=%async_computation.1 | async-start | bytes 6291456 | tf_op jit(solution)/shard_map/all_gather | solution.py:89
  11.3 1.4 copy-start.4
  11.3 105.4 %all-gather.22.cloned.1.call-start = ((), (), s32[]{:S(2)}) async-start(), calls=%async_computation.7 | async-start | bytes 2621440 | tf_op jit(solution)/shard_map/all_gather | solution.py:83
  12.0 128.6 %all-gather.12.cloned.1.call-start = ((), (), s32[]{:S(2)}) async-start(), calls=%async_computation.2 | async-start | bytes 2621440 | tf_op jit(solution)/shard_map/all_gather | solution.py:80
  12.6 152.1 %all-gather.20.cloned.1.call-start = ((), (), s32[]{:S(2)}) async-start(), calls=%async_computation.6 | async-start | bytes 2621440 | tf_op jit(solution)/shard_map/all_gather | solution.py:81
  13.7 175.0 %all-gather.14.cloned.1.call-start = ((), (), s32[]{:S(2)}) async-start(), calls=%async_computation.3 | async-start | bytes 2621440 | tf_op jit(solution)/shard_map/all_gather | solution.py:84
  14.3 256.7 %all-gather.18.cloned.1.call-start = ((), (), s32[]{:S(2)}) async-start(), calls=%async_computation.5 | async-start | bytes 5242880 | tf_op jit(solution)/shard_map/all_gather | solution.py:138
  98.7 25.0 %copy-start.8 = (f32[1024]{0:T(1024)S(1)}, f32[1024]{0:T(1024)}, u32[]{:S(2)}) copy-start(f32[1024]{0:T(1024)} %param.19) | copy-start | bytes 12292
  98.7 25.7 %copy-start.5 = (f32[2,4,2048]{2,1,0:T(4,128)S(1)}, f32[2,4,2048]{2,1,0:T(4,128)}, u32[]{:S(2)}) copy-start(f32[2,4,2048]{2,1,0:T(4,128)} %param.23) | copy-start | bytes 196612
  98.7 253.1 %all-gather.24.cloned.1.call-start = ((), (), s32[]{:S(2)}) async-start(), calls=%async_computation.8 | async-start | bytes 5242880 | tf_op jit(solution)/shard_map/all_gather | solution.py:139
  122.9 255.9 %all-gather.26.cloned.1.call-start = ((), (), s32[]{:S(2)}) async-start(), calls=%async_computation.9 | async-start | bytes 2621440 | tf_op jit(solution)/shard_map/all_gather | solution.py:85
  123.6 352.8 %reduce-scatter.2.cloned.1.call-start = ((), (), s32[]{:S(2)}) async-start(), calls=%async_computation.10 | async-start | bytes 6291456 | tf_op jit(solution)/shard_map/reduce_scatter | solution.py:196
  145.9 27.6 %collective-permute-start = (bf16[2,15,512]{2,1,0:T(8,128)(2,1)S(1)}, bf16[2,15,512]{2,1,0:T(8,128)(2,1)}, u32[]{:S(2)}, u32[]{:S(2)}) collective-permute-start(bf16[2,15,512]{2,1,0:T(8,128)(2,1)S(1)} %slice.84), channel_id=1, source_target_pairs={{0,8},{8,16},{16,24},{1,9},{9,17},{17,25},{2,10},{10,18},{18,26},{... | collective-permute-start | bytes 92168 | tf_op jit(solution)/shard_map/ppermute | solution.py:16
  182.5 1.5 copy-start.7
  358.2 1.3 copy-start.3
  387.2 89.2 %copy-start.1 = (bf16[8,128,128]{2,1,0:T(8,128)(2,1)S(1)}, bf16[8,128,128]{2,1,0:T(8,128)(2,1)}, u32[]{:S(2)}) copy-start(bf16[8,128,128]{2,1,0:T(8,128)(2,1)} %param.18) | copy-start | bytes 786436
Sparse Core Ops, SparseCore 0:
  8.9 25.2 all-gather.15
  35.8 56.7 all-gather.9
  94.1 22.5 all-gather.21
  118.1 22.5 all-gather.11
  142.1 22.5 all-gather.19
  166.1 22.5 all-gather.13
  190.3 80.7 all-gather.17
  272.6 79.2 all-gather.23
  353.4 21.0 all-gather.25
  387.3 89.0 reduce-scatter.1
where the time goes:
time: 484 us; the launch traced here: 483 us
  waiting for transfers between devices  374 us (77%)
  matrix products  47.3 us (10%)
  local copies, waits for them, and re-layouts  27 us (6%)
  other arithmetic  13.8 us (3%)
  between operations  13.8 us (3%)
    reduce_scatter x1, waiting for transfers between devices, on_device(): lax.psum_scatter((jnp.dot(pool_flat, out_pool_full, preferred_element_typ...  89.2 us
    all_gather x1, waiting for transfers between devices, on_device(): key_shard = lax.all_gather(key_proj, 'sp', axis=1, tiled=True)  75.1 us
    all_gather x1, waiting for transfers between devices, on_device(): value_shard = lax.all_gather(value_proj, 'sp', axis=1, tiled=True)  74.5 us
    all_gather x1, waiting for transfers between devices, on_device(): shard_rows = lax.all_gather(normed, 'tp', axis=1, tiled=True)  58.3 us
    all_gather x1, waiting for transfers between devices, on_device(): lax.all_gather(w_key, 'fs', axis=0, tiled=True)  19.8 us
    all_gather x1, waiting for transfers between devices, on_device(): lax.all_gather(w_value, 'fs', axis=0, tiled=True)  17.9 us
    unnamed x22, local copies, waits for them, and re-layouts  17 us
    all_gather x1, waiting for transfers between devices, on_device(): lax.all_gather(w_pool_in, 'fs', axis=0, tiled=True)  16.3 us
  transfers between devices with their start and end apart: 11, of which 9 were waited for; matrix products, arithmetic and copies ran while one was open for 16% of the time, Pallas kernels for 0%

commit v1 on v0

--- a/solution.py
+++ b/solution.py
@@ -136,7 +136,12 @@
         jnp.zeros((seq_count, token_count, head_count, HEAD_DIM), jnp.float32),
     )
     key_shard = lax.all_gather(key_proj, "sp", axis=1, tiled=True)
-    value_shard = lax.all_gather(value_proj, "sp", axis=1, tiled=True)
+    ring = [value_proj]
+    for hop in range(3):
+        ring.append(lax.ppermute(ring[-1], "sp", [(dev, (dev + 1) % 4) for dev in range(4)]))
+    value_shard = jnp.roll(
+        jnp.concatenate(ring[::-1], axis=1), (lax.axis_index("sp") + 1) * ring[0].shape[1], axis=1
+    )
     key_total = key_shard.shape[1]
     block_rows = 512
 

time: 484 us -> 427 us (0.88)
  waiting for transfers between devices: 374 us -> 298 us
  local copies, waits for them, and re-layouts: 27 us -> 40.8 us
  starting transfers between devices: 4.34 us -> 9.66 us
    all_gather x1 -> x0, waiting for transfers between devices: 74.5 us -> none  [on_device(): value_shard = lax.all_gather(value_proj, 'sp', axis=1, tiled=True)]
    ppermute x0 -> x3, waiting for transfers between devices: none -> 57.6 us  [on_device(): lax.ppermute(ring[-1], 'sp', [(dev, (dev + 1) % 4) for dev in range(4)])]
    all_gather x1, waiting for transfers between devices: 75.1 us -> 22.1 us  [on_device(): key_shard = lax.all_gather(key_proj, 'sp', axis=1, tiled=True)]
    unnamed x22 -> x35, local copies, waits for them, and re-layouts: 17 us -> 24.3 us
    ppermute x0 -> x3, starting transfers between devices: none -> 5.36 us  [on_device(): lax.ppermute(ring[-1], 'sp', [(dev, (dev + 1) % 4) for dev in range(4)])]
  transfers between devices with their start and end apart: 11 -> 13, of which waited for: 9 -> 9; matrix products, arithmetic and copies ran while one was open for 16% -> 21% of each run, Pallas kernels for 0% -> 0%
where the time goes in v1:
time: 427 us; the launch traced here: 426 us
  waiting for transfers between devices  298 us (70%)
  matrix products  46.3 us (11%)
  local copies, waits for them, and re-layouts  40.8 us (10%)
  other arithmetic  14.2 us (3%)
  between operations  13.6 us (3%)
  starting transfers between devices  9.66 us (2%)
    reduce_scatter x1, waiting for transfers between devices, on_device(): lax.psum_scatter((jnp.dot(pool_flat, out_pool_full, preferred_element_typ...  89.5 us
    all_gather x1, waiting for transfers between devices, on_device(): shard_rows = lax.all_gather(normed, 'tp', axis=1, tiled=True)  58.3 us
    ppermute x3, waiting for transfers between devices, on_device(): lax.ppermute(ring[-1], 'sp', [(dev, (dev + 1) % 4) for dev in range(4)])  57.6 us
    unnamed x35, local copies, waits for them, and re-layouts  24.3 us
    all_gather x1, waiting for transfers between devices, on_device(): key_shard = lax.all_gather(key_proj, 'sp', axis=1, tiled=True)  22.1 us
    all_gather x1, waiting for transfers between devices, on_device(): lax.all_gather(w_key, 'fs', axis=0, tiled=True)  19.9 us
    all_gather x1, waiting for transfers between devices, on_device(): lax.all_gather(w_value, 'fs', axis=0, tiled=True)  18.5 us
    all_gather x1, waiting for transfers between devices, on_device(): lax.all_gather(w_pool_in, 'fs', axis=0, tiled=True)  16.4 us
  transfers between devices with their start and end apart: 13, of which 9 were waited for; matrix products, arithmetic and copies ran while one was open for 21% of the time, Pallas kernels for 0%

profile of v1, /device:TPU:0, one launch (start us, length us, event | category | flops | bytes accessed | tf_op | source)
XLA Modules:
  0.0 425.9 jit_solution(4818338535322762356)
XLA Ops:
  14.4 19.9 %all-gather.15.cloned.1.call-done = bf16[2048,512]{1,0:T(8,128)(2,1)} async-done(((bf16[512,512]{1,0:T(8,128)(2,1)}), bf16[2048,512]{1,0:T(8,128)(2,1)}) %all-gather.15.cloned.1.call-update) | async-done | bytes 2097168 | tf_op jit(solution)/shard_map/all_gather | solution.py:82
  34.2 58.3 %all-gather.9.cloned.1.call-done = bf16[2,512,2048]{2,1,0:T(8,128)(2,1)} async-done(((bf16[2,256,2048]{2,1,0:T(8,128)(2,1)}), bf16[2,512,2048]{2,1,0:T(8,128)(2,1)}) %all-gather.9.cloned.1.call-update) | async-done | bytes 4194320 | tf_op jit(solution)/shard_map/all_gather | solution.py:89
  92.5 6.2 %fusion.29 = bf16[2,512,512]{2,1,0:T(8,128)(2,1)} fusion(bf16[2,512,2048]{2,1,0:T(8,128)(2,1)} %all-gather.9.cloned.1.call-done, bf16[2048,512]{1,0:T(8,128)(2,1)} %all-gather.15.cloned.1.call-done), kind=kOutput, calls=%fused_computation.42 | convolution fusion | flops 2148007936 | bytes 7340032 | tf_op jit(solution)/shard_map/dot_general | solution.py:96
  100.3 16.4 %all-gather.11.cloned.1.call-done = bf16[2048,512]{1,0:T(8,128)(2,1)} async-done(((bf16[512,512]{1,0:T(8,128)(2,1)}), bf16[2048,512]{1,0:T(8,128)(2,1)}) %all-gather.11.cloned.1.call-update) | async-done | bytes 2097168 | tf_op jit(solution)/shard_map/all_gather | solution.py:80
  116.7 5.2 %fusion.26 = bf16[2,512,512]{2,1,0:T(8,128)(2,1)S(1)} fusion(bf16[2,512,2048]{2,1,0:T(8,128)(2,1)} %all-gather.9.cloned.1.call-done, bf16[2048,512]{1,0:T(8,128)(2,1)} %all-gather.11.cloned.1.call-done), kind=kOutput, calls=%fused_computation.41 | convolution fusion | flops 2148007936 | bytes 7340032 | tf_op jit(solution)/shard_map/dot_general | solution.py:92
  122.2 18.5 %all-gather.21.cloned.1.call-done = bf16[2048,512]{1,0:T(8,128)(2,1)} async-done(((bf16[512,512]{1,0:T(8,128)(2,1)}), bf16[2048,512]{1,0:T(8,128)(2,1)}) %all-gather.21.cloned.1.call-update) | async-done | bytes 2097168 | tf_op jit(solution)/shard_map/all_gather | solution.py:83
  140.7 6.2 %fusion.35 = bf16[2,512,512]{2,1,0:T(8,128)(2,1)} fusion(bf16[2,512,2048]{2,1,0:T(8,128)(2,1)} %all-gather.9.cloned.1.call-done, bf16[2048,512]{1,0:T(8,128)(2,1)} %all-gather.21.cloned.1.call-done), kind=kOutput, calls=%fused_computation.44 | convolution fusion | flops 2148007936 | bytes 7340032 | tf_op jit(solution)/shard_map/dot_general | solution.py:97
  148.4 4.0 collective-permute-start
  152.4 12.3 %all-gather.19.cloned.1.call-done = bf16[2048,512]{0,1:T(8,128)(2,1)} async-done(((bf16[512,512]{0,1:T(8,128)(2,1)}), bf16[2048,512]{0,1:T(8,128)(2,1)}) %all-gather.19.cloned.1.call-update) | async-done | bytes 2097168 | tf_op jit(solution)/shard_map/all_gather | solution.py:81
  164.7 6.2 %fusion.32 = bf16[2,512,512]{1,2,0:T(8,128)(2,1)} fusion(bf16[2,512,2048]{2,1,0:T(8,128)(2,1)} %all-gather.9.cloned.1.call-done, bf16[2048,512]{0,1:T(8,128)(2,1)} %all-gather.19.cloned.1.call-done), kind=kOutput, calls=%fused_computation.43 | convolution fusion | flops 2148007936 | bytes 7340032 | tf_op jit(solution)/shard_map/dot_general | solution.py:93
  170.9 2.3 copy.39
  180.8 25.2 %collective-permute-done.2 = bf16[2,512,512]{2,1,0:T(8,128)(2,1)} collective-permute-done((bf16[2,512,512]{2,1,0:T(8,128)(2,1)}, bf16[2,512,512]{2,1,0:T(8,128)(2,1)}, u32[]{:S(2)}, u32[]{:S(2)}) %collective-permute-start.2) | collective-permute-done | bytes 1048608 | tf_op jit(solution)/shard_map/ppermute | solution.py:141
  216.4 7.3 %fusion.79 = f32[1024,2048]{1,0:T(8,128)} fusion(bf16[1024,512]{1,0:T(8,128)(2,1)S(1)} %bitcast.129, bf16[512,2048]{1,0:T(8,128)(2,1)} %all-gather.13.cloned.1.call-done), kind=kOutput, calls=%fused_computation.132 | convolution fusion | flops 2147483648 | bytes 11534336 | tf_op jit(solution)/shard_map/dot_general | solution.py:203
  223.7 32.4 %collective-permute-done.3 = bf16[2,512,512]{2,1,0:T(8,128)(2,1)S(1)} collective-permute-done((bf16[2,512,512]{2,1,0:T(8,128)(2,1)}, bf16[2,512,512]{2,1,0:T(8,128)(2,1)S(1)}, u32[]{:S(2)}, u32[]{:S(2)}) %collective-permute-start.3) | collective-permute-done | bytes 1048608 | tf_op jit(solution)/shard_map/ppermute | solution.py:141
  266.3 6.3 %copy.40 = bf16[2,2048,512]{1,2,0:T(8,128)(2,1)} copy(bf16[2,2048,512]{2,1,0:T(8,128)(2,1)} %constant_dynamic-slice_fusion.3) | data formatting | bytes 8388608
  272.6 22.1 %all-gather.17.cloned.1.call-done = bf16[2,2048,512]{2,1,0:T(8,128)(2,1)} async-done(((bf16[2,512,512]{2,1,0:T(8,128)(2,1)}), bf16[2,2048,512]{2,1,0:T(8,128)(2,1)}) %all-gather.17.cloned.1.call-update) | async-done | bytes 4194320 | tf_op jit(solution)/shard_map/all_gather | solution.py:138
  294.7 6.2 %copy.38 = bf16[2,2048,512]{1,2,0:T(8,128)(2,1)} copy(bf16[2,2048,512]{2,1,0:T(8,128)(2,1)} %all-gather.17.cloned.1.call-done) | data formatting | bytes 8388608
  302.2 17.2 %while.15 = (s32[]{:T(128)}, f32[2,512,4]{1,2,0:T(4,128)S(1)}, f32[2,512,4]{1,2,0:T(4,128)S(1)}, f32[2,512,4,128]{1,3,2,0:T(8,128)S(1)}, s32[4]{0:T(128)S(1)}, /...) while((s32[]{:T(128)}, f32[2,512,4]{1,2,0:T(4,128)S(1)}, ...), condition=%wide.region_6.7_spmd.clone, body=%wide.region_1.6_spmd.clone.sunk | while | flops 1114907648 | bytes 38154656 | solution.py:188
  303.5 12.0 %conditional.3 = ((f32[2,512,4]{1,2,0:T(4,128)S(1)}, f32[2,512,4]{1,2,0:T(4,128)S(1)}, f32[2,512,4,128]{1,3,2,0:T(8,128)S(1)})) conditional(s32[]{:T(128)} %convert_element_type.217, (f32[2,512,4]{1,2,0:T(4,128)S(1)}, f32[2,512,4]{1,2,0:T(4,128)S(1)}, f32[2,512,4,128]{1,3,2,0:T(8,128)S(1)}) %tuple.49, (s32[]{:T(128)}, s32[]{:T(128)}, s32[]{:T(128)}, ...), branch_computations={%region_2.2_spmd, %region_3.5_spmd} | conditional | flops 1114907648 | bytes 38152320 | solution.py:186
  306.1 2.6 fusion.6
  308.8 3.2 fusion.5
  312.0 3.5 bitcast_add_fusion.1
  321.5 8.4 %add_convert_fusion = bf16[1024,2048]{1,0:T(8,128)(2,1)} fusion(f32[1024,2048]{1,0:T(8,128)} %fusion.79, bf16[1024,512]{1,0:T(8,128)(2,1)S(1)} %bitcast.130, bf16[512,2048]{1,0:T(8,128)(2,1)} %all-gather.23.cloned.1.call-done), kind=kOutput, calls=%fused_computation.22 | convolution fusion | flops 2151677952 | bytes 15728640 | tf_op jit(solution)/shard_map/dot_general | solution.py:204
  329.9 89.5 %reduce-scatter.2.cloned.1.call-done = bf16[512,2048]{1,0:T(8,128)(2,1)} async-done(((bf16[1024,2048]{1,0:T(8,128)(2,1)}), bf16[512,2048]{1,0:T(8,128)(2,1)}) %reduce-scatter.2.cloned.1.call-update) | async-done | bytes 2097168 | tf_op jit(solution)/shard_map/reduce_scatter | solution.py:201
  (115 shorter events, 46.7 us)
Async XLA Ops:
  6.5 173.9 %copy-start = (bf16[8,128,128]{2,1,0:T(8,128)(2,1)S(1)}, bf16[8,128,128]{2,1,0:T(8,128)(2,1)}, u32[]{:S(2)}) copy-start(bf16[8,128,128]{2,1,0:T(8,128)(2,1)} %param.18) | copy-start | bytes 786436
  6.5 2.9 copy-start.4
  6.5 2.9 copy-start.9
  6.5 27.7 %all-gather.15.cloned.1.call-start = ((), (), s32[]{:S(2)}) async-start(), calls=%async_computation.4 | async-start | bytes 2621440 | tf_op jit(solution)/shard_map/all_gather | solution.py:82
  7.3 85.2 %all-gather.9.cloned.1.call-start = ((), (), s32[]{:S(2)}) async-start(), calls=%async_computation.1 | async-start | bytes 6291456 | tf_op jit(solution)/shard_map/all_gather | solution.py:89
  11.3 1.4 copy-start.7
  11.3 105.4 %all-gather.11.cloned.1.call-start = ((), (), s32[]{:S(2)}) async-start(), calls=%async_computation.2 | async-start | bytes 2621440 | tf_op jit(solution)/shard_map/all_gather | solution.py:80
  12.0 128.6 %all-gather.21.cloned.1.call-start = ((), (), s32[]{:S(2)}) async-start(), calls=%async_computation.7 | async-start | bytes 2621440 | tf_op jit(solution)/shard_map/all_gather | solution.py:83
  12.6 152.1 %all-gather.19.cloned.1.call-start = ((), (), s32[]{:S(2)}) async-start(), calls=%async_computation.6 | async-start | bytes 2621440 | tf_op jit(solution)/shard_map/all_gather | solution.py:81
  13.7 202.7 %all-gather.13.cloned.1.call-start = ((), (), s32[]{:S(2)}) async-start(), calls=%async_computation.3 | async-start | bytes 2621440 | tf_op jit(solution)/shard_map/all_gather | solution.py:84
  14.3 85.3 %copy-start.8 = (f32[2,4,2048]{2,1,0:T(4,128)S(1)}, f32[2,4,2048]{2,1,0:T(4,128)}, u32[]{:S(2)}) copy-start(f32[2,4,2048]{2,1,0:T(4,128)} %param.23) | copy-start | bytes 196612
  14.3 85.4 %copy-start.11 = (f32[1024]{0:T(1024)S(1)}, f32[1024]{0:T(1024)}, u32[]{:S(2)}) copy-start(f32[1024]{0:T(1024)} %param.19) | copy-start | bytes 12292
  14.3 280.4 %all-gather.17.cloned.1.call-start = ((), (), s32[]{:S(2)}) async-start(), calls=%async_computation.5 | async-start | bytes 5242880 | tf_op jit(solution)/shard_map/all_gather | solution.py:138
  98.7 222.7 %all-gather.23.cloned.1.call-start = ((), (), s32[]{:S(2)}) async-start(), calls=%async_computation.8 | async-start | bytes 2621440 | tf_op jit(solution)/shard_map/all_gather | solution.py:85
  99.5 319.9 %reduce-scatter.2.cloned.1.call-start = ((), (), s32[]{:S(2)}) async-start(), calls=%async_computation.9 | async-start | bytes 6291456 | tf_op jit(solution)/shard_map/reduce_scatter | solution.py:201
  146.9 29.7 %collective-permute-start.1 = (bf16[2,512,512]{2,1,0:T(8,128)(2,1)}, bf16[2,512,512]{2,1,0:T(8,128)(2,1)}, u32[]{:S(2)}, u32[]{:S(2)}) collective-permute-start(bf16[2,512,512]{2,1,0:T(8,128)(2,1)} %fusion.35), channel_id=1, source_target_pairs={{0,8},{8,16},{16,24},{24,0},{1,9},{9,17},{17,25},{25,1},{2,10},{10... | collective-permute-start | bytes 3145736 | tf_op jit(solution)/shard_map/ppermute | solution.py:141
  148.4 24.8 %collective-permute-start = (bf16[2,15,512]{2,1,0:T(8,128)(2,1)S(1)}, bf16[2,15,512]{2,1,0:T(8,128)(2,1)}, u32[]{:S(2)}, u32[]{:S(2)}) collective-permute-start(bf16[2,15,512]{2,1,0:T(8,128)(2,1)S(1)} %slice.84), channel_id=1, source_target_pairs={{0,8},{8,16},{16,24},{1,9},{9,17},{17,25},{2,10},{10,18},{18,26},{... | collective-permute-start | bytes 92168 | tf_op jit(solution)/shard_map/ppermute | solution.py:16
  176.3 2.0 copy-start.3
  176.3 2.0 slice-start
  176.6 29.5 %collective-permute-start.2 = (bf16[2,512,512]{2,1,0:T(8,128)(2,1)}, bf16[2,512,512]{2,1,0:T(8,128)(2,1)}, u32[]{:S(2)}, u32[]{:S(2)}) collective-permute-start(bf16[2,512,512]{2,1,0:T(8,128)(2,1)} %collective-permute-done.1), channel_id=1, source_target_pairs={{0,8},{8,16},{16,24},{24,0},{1,9},{9,17},{17,25},{25,1},{2,10},{10... | collective-permute-start | bytes 3145736 | tf_op jit(solution)/shard_map/ppermute | solution.py:141
  206.1 50.0 %collective-permute-start.3 = (bf16[2,512,512]{2,1,0:T(8,128)(2,1)}, bf16[2,512,512]{2,1,0:T(8,128)(2,1)S(1)}, u32[]{:S(2)}, u32[]{:S(2)}) collective-permute-start(bf16[2,512,512]{2,1,0:T(8,128)(2,1)} %collective-permute-done.2), channel_id=1, source_target_pairs={{0,8},{8,16},{16,24},{24,0},{1,9},{9,17},{17,25},{25,1},{2,10},{10... | collective-permute-start | bytes 3145736 | tf_op jit(solution)/shard_map/ppermute | solution.py:141
  212.5 2.3 copy-start.10
  213.2 1.6 copy-start.5
  329.9 89.5 %copy-start.1 = (bf16[8,128,128]{2,1,0:T(8,128)(2,1)S(1)}, bf16[8,128,128]{2,1,0:T(8,128)(2,1)}, u32[]{:S(2)}) copy-start(bf16[8,128,128]{2,1,0:T(8,128)(2,1)} %param.18) | copy-start | bytes 786436
  (2 other events, 2.3 us)
Sparse Core Ops, SparseCore 0:
  8.9 25.2 all-gather.14
  35.8 56.7 all-gather.8
  94.1 22.5 all-gather.10
  118.1 22.5 all-gather.20
  142.1 22.5 all-gather.18
  166.1 22.5 all-gather.12
  190.3 104.3 all-gather.16
  296.2 20.4 all-gather.22
  330.1 89.2 reduce-scatter.1
